TPU v7x, 32 devices: a whole 2x2x4 slice. The times are simulated.
32 devices in a mesh: ep: 8 (over z, x), tp: 4 (over y, core).
Axes of the slice: x: 2, y: 2, z: 4, core: 2. Of those that a mesh axis runs over, the one named last changes fastest.
Arguments:
- query_rows: bfloat16 [1536, 1024], P('ep', 'tp'), may hold values from -8 to 8
- key_rows: bfloat16 [1536, 1024], P('ep', 'tp'), may hold values from -8 to 8
- value_rows: bfloat16 [1536, 1024], P('ep', 'tp'), may hold values from -6 to 6
- lambdas: float32 [8], P('tp'), may hold values from 0.3 to 0.8
- head_gain: float32 [128], replicated, may hold values from 0.1 to 1.9
- w_out: bfloat16 [1024, 2048], replicated, may hold values from -0.1875 to 0.1875
- moe_rows: bfloat16 [4096, 2048], P('ep'), may hold values from -6 to 6
- ffn_gain: float32 [2048], replicated, may hold values from 0.1 to 1.9
- routes: int32 [4096, 2], P('ep'), may hold values from 0 to 7, all different within a row; in each aligned block of 128 rows (0 to 127, 128 to 255, ...) at most 64 rows name the same one
- group_logits: float32 [4096, 4], P('ep'), may hold values from -8 to 8
- pick_logits: float32 [4096, 2], P('ep'), may hold values from -8 to 8
- w_gate: bfloat16 [8, 2048, 1024], P('ep', None, 'tp'), may hold values from -0.125 to 0.125
- w_up: bfloat16 [8, 2048, 1024], P('ep', None, 'tp'), may hold values from -0.125 to 0.125
- w_down: bfloat16 [8, 1024, 2048], P('ep', 'tp'), may hold values from -0.75 to 0.75
Outputs:
- mixer_out: bfloat16 [1536, 2048], P(('ep', 'tp'))
- moe_out: bfloat16 [4096, 2048], P(('ep', 'tp'))
Inputs may be any that keep to these rules, and one draw needn't show every extreme that they name: `routes`: each row names 2 different experts. In each aligned block of 128 rows (the rows of one device) no expert is named by more than 64 rows; some expert is named by exactly 64 rows of a block.
All inputs are finite; a program needn't handle non-finite values.
Results may differ from a plain program's by a relative error of at most 0.015.
Values may be sent and summed in bfloat16 or wider, within the bound.
A program may use at most 128 MiB of HBM per device.

v0:
```python
import jax
import jax.numpy as jnp
from jax import lax
from jax.sharding import PartitionSpec as P

EPS = 1e-06
HEAD_SCALE = 0.8


def rms_rows(values, gain):
    squared = jnp.mean(values * values, axis=-1, keepdims=True)
    return values * lax.rsqrt(squared + EPS) * gain


def slot_index(picks, expert_count, capacity):
    flattened = picks.reshape(picks.shape[0], -1)
    onehot = (flattened[..., None] == jnp.arange(expert_count, dtype=jnp.int32)).astype(jnp.int32)
    before = jnp.cumsum(onehot, axis=1) - onehot
    ranking = jnp.sum(before * onehot, axis=-1)
    return flattened * capacity + ranking


def expert_hidden(arrived, gate_weight, up_weight):
    gate_part = jnp.dot(arrived, gate_weight, preferred_element_type=jnp.float32)
    up_part = jnp.dot(arrived, up_weight, preferred_element_type=jnp.float32)
    return (jax.nn.silu(gate_part) * up_part).astype(jnp.bfloat16)


def local(
    query_rows,
    key_rows,
    value_rows,
    lambdas,
    head_gain,
    w_out,
    moe_rows,
    ffn_gain,
    routes,
    group_logits,
    pick_logits,
    w_gate,
    w_up,
    w_down,
):
    token_count = query_rows.shape[0]
    local_heads = lambdas.shape[0]
    head_qk = query_rows.shape[1] // (2 * local_heads)
    head_v = value_rows.shape[1] // local_heads
    score_scale = head_qk ** (-0.5)
    queries = query_rows.reshape(token_count, local_heads, 2, head_qk)

    def absorb(carried, key_value):
        key_block, value_block = key_value
        running_max, running_sum, running_acc = carried
        scores = (
            jnp.einsum("qhmd,khmd->hmqk", queries, key_block, preferred_element_type=jnp.float32)
            * score_scale
        )
        new_max = jnp.maximum(running_max, jnp.max(scores, axis=-1))
        factor = jnp.exp(running_max - new_max)
        weights = jnp.exp(scores - new_max[..., None])
        running_sum = running_sum * factor + jnp.sum(weights, axis=-1)
        update = jnp.einsum(
            "hmqk,khv->hmqv",
            weights.astype(jnp.bfloat16),
            value_block,
            preferred_element_type=jnp.float32,
        )
        return ((new_max, running_sum, running_acc * factor[..., None] + update), None)

    start_state = (
        jnp.full((local_heads, 2, token_count), -1e30, jnp.float32),
        jnp.zeros((local_heads, 2, token_count), jnp.float32),
        jnp.zeros((local_heads, 2, token_count, head_v), jnp.float32),
    )
    carried = start_state
    key_piece = lax.all_gather(key_rows, "ep", axis=0, tiled=True)
    value_piece = lax.all_gather(value_rows, "ep", axis=0, tiled=True)
    length = key_piece.shape[0]
    block_rows = 1024 if length % 1024 == 0 else length
    blocks = (
        key_piece.reshape(length // block_rows, block_rows, local_heads, 2, head_qk),
        value_piece.reshape(length // block_rows, block_rows, local_heads, head_v),
    )
    carried, unused = lax.scan(absorb, carried, blocks)
    unused_max, final_sum, final_acc = carried
    averaged = final_acc / final_sum[..., None]
    per_head = averaged[:, 0] - lambdas[:, None, None] * averaged[:, 1]
    normed_heads = rms_rows(per_head, head_gain) * HEAD_SCALE
    attended = (
        jnp.transpose(normed_heads, (1, 0, 2))
        .reshape(token_count, local_heads * head_v)
        .astype(jnp.bfloat16)
    )
    own_weight = lax.dynamic_slice_in_dim(
        w_out, lax.axis_index("tp") * attended.shape[1], attended.shape[1], 0
    )
    mixer_out = lax.psum_scatter(
        jnp.dot(attended, own_weight, preferred_element_type=jnp.float32).astype(jnp.bfloat16),
        "tp",
        scatter_dimension=0,
        tiled=True,
    )
    quarters = lax.axis_size("tp")
    own_quarter = lax.axis_index("tp")
    expert_count = lax.axis_size("ep")
    model_width = moe_rows.shape[1]
    quarter_rows = moe_rows.shape[0] // quarters
    top_k = routes.shape[1]
    capacity = max(2, 2 * top_k * quarter_rows // expert_count)
    source_rows = jnp.repeat(jnp.arange(quarter_rows, dtype=jnp.int32), top_k)
    own_picks = lax.dynamic_slice_in_dim(routes, own_quarter * quarter_rows, quarter_rows, 0)
    own_tokens = lax.dynamic_slice_in_dim(moe_rows, own_quarter * quarter_rows, quarter_rows, 0)
    normed = rms_rows(own_tokens.astype(jnp.float32), ffn_gain).astype(jnp.bfloat16)
    own_slots = slot_index(own_picks[None], expert_count, capacity)[0]
    outgoing = (
        jnp.zeros((expert_count * capacity, model_width), jnp.bfloat16)
        .at[own_slots]
        .set(normed[source_rows])
    )
    arrived = lax.all_to_all(
        outgoing.reshape(expert_count, capacity, model_width),
        "ep",
        split_axis=0,
        concat_axis=0,
        tiled=True,
    )
    pieces = lax.all_gather(arrived, "tp", axis=0, tiled=True)
    flat_rows = pieces.reshape(-1, model_width)
    hidden = expert_hidden(flat_rows, w_gate[0], w_up[0]).reshape(pieces.shape[0], capacity, -1)
    hidden_flat = hidden.reshape(-1, hidden.shape[-1])
    summed = lax.psum_scatter(
        jnp.dot(hidden_flat, w_down[0], preferred_element_type=jnp.float32).astype(jnp.bfloat16),
        "tp",
        scatter_dimension=0,
        tiled=True,
    )
    returned = lax.all_to_all(
        summed.reshape(expert_count, capacity, model_width),
        "ep",
        split_axis=0,
        concat_axis=0,
        tiled=True,
    )
    picked = returned.reshape(-1, model_width)[own_slots].reshape(quarter_rows, top_k, model_width)
    own_groups = lax.dynamic_slice_in_dim(group_logits, own_quarter * quarter_rows, quarter_rows, 0)
    own_pick_logits = lax.dynamic_slice_in_dim(
        pick_logits, own_quarter * quarter_rows, quarter_rows, 0
    )
    group_count = group_logits.shape[1]
    group_prob = jax.nn.softmax(own_groups, axis=-1)
    group_index = own_picks // (expert_count // group_count)
    matches = (group_index[..., None] == jnp.arange(group_count, dtype=jnp.int32)).astype(
        jnp.float32
    )
    group_share = jnp.sum(group_prob[:, None, :] * matches, axis=-1)
    gate_values = group_share * jax.nn.softmax(own_pick_logits, axis=-1)
    moe_out = jnp.sum(gate_values[..., None] * picked.astype(jnp.float32), axis=1).astype(
        jnp.bfloat16
    )
    return (mixer_out, moe_out)


def solution(mesh):
    return jax.shard_map(
        local,
        mesh=mesh,
        in_specs=(
            P("ep", "tp"),
            P("ep", "tp"),
            P("ep", "tp"),
            P("tp"),
            P(),
            P(),
            P("ep", None),
            P(),
            P("ep", None),
            P("ep", None),
            P("ep", None),
            P("ep", None, "tp"),
            P("ep", None, "tp"),
            P("ep", "tp", None),
        ),
        out_specs=(P(("ep", "tp"), None), P(("ep", "tp"), None)),
        check_vma=False,
    )
```

profile of v0, /device:TPU:0, one launch (start us, length us, event | category | flops | bytes accessed | tf_op | source)
XLA Modules:
  0.0 339.7 jit_solution(261808291416860606)
XLA Ops:
  7.2 0.0 copy-start
  7.2 0.0 all-gather.2.cloned.1.call-start
  7.2 0.8 and_select_fusion
  8.0 0.1 copy.52
  8.1 0.1 eq.43
  8.3 0.6 reduce-window.6
  8.9 0.2 slice_reduce_fusion
  9.1 0.1 fusion.32
  9.2 0.1 copy.51
  9.3 0.1 mul.152
  9.5 0.1 reshape.255
  9.6 1.2 fusion.10
  10.9 2.0 fusion.12
  12.9 6.2 %scatter_custom_fusion = bf16[512,2048]{1,0:T(8,128)(2,1)S(1)} fusion(s32[256]{0:T(256)S(1)} %bitcast.82, bf16[128,2048]{1,0:T(8,128)(2,1)} %fusion.12, s32[1024]{0:T(1024)S(1)} %pad_clamp_fusion.1, bf16[]{:T(256)} %constant.73.clone.1), kind=kCustom, calls=%fused_computation.25 | custom fusion | bytes 2097664 | tf_op jit(solution)/shard_map/scatter | solution.py:119
  19.2 55.4 %all_to_all.10 = bf16[8,64,2048]{2,1,0:T(8,128)(2,1)} all-to-all(bf16[8,64,2048]{2,1,0:T(8,128)(2,1)S(1)} %bitcast.77), channel_id=1, replica_groups=mesh['ep'=8,'tp'=4] {'ep'}, dimensions={0} | all-to-all | bytes 4194304 | tf_op jit(solution)/shard_map/all_to_all | solution.py:121
  74.6 0.0 all-gather.2.cloned.1.call-update
  74.6 0.2 reduce-scatter.5.cloned.1.call-start
  74.9 57.2 %all-gather.2.cloned.1.call-done = bf16[32,64,2048]{2,1,0:T(8,128)(2,1)} async-done(((bf16[8,64,2048]{2,1,0:T(8,128)(2,1)}), bf16[32,64,2048]{2,1,0:T(8,128)(2,1)}) %all-gather.2.cloned.1.call-update) | async-done | bytes 8388624 | tf_op jit(solution)/shard_map/all_gather | solution.py:128
  132.1 0.0 copy-start.9
  132.1 7.4 %fusion.16 = f32[2048,256]{1,0:T(8,128)} fusion(bf16[2048,2048]{1,0:T(8,128)(2,1)} %bitcast.87, bf16[1,2048,256]{2,1,0:T(8,128)(2,1)} %param.25), kind=kOutput, calls=%fused_computation.23 | convolution fusion | flops 2147483648 | bytes 11534336 | tf_op jit(solution)/shard_map/dot_general | solution.py:24
  139.5 0.0 copy-done
  139.5 0.0 copy-done.9
  139.5 13.2 %convolution_convert_fusion = bf16[2048,2048]{1,0:T(8,128)(2,1)} fusion(bf16[2048,2048]{1,0:T(8,128)(2,1)} %bitcast.88, f32[2048,256]{1,0:T(8,128)} %fusion.16, bf16[1,256,2048]{2,1,0:T(8,128)(2,1)S(1)} %copy-done, bf16[1,2048,256]{2,1,0:T(8,128)(2,1)S(1)} %copy-done.9), kind=kOutput, calls=%fused_computation.3 | convolution fusion | flops 4302307328 | bytes 20971520 | tf_op jit(solution)/shard_map/dot_general | solution.py:133
  152.7 0.0 copy-start.2
  152.7 0.0 reduce-scatter.5.cloned.1.call-update
  152.7 0.9 copy-done.2
  153.5 0.0 copy-start.3
  153.6 32.4 %all_gather.9 = bf16[1536,256]{1,0:T(8,128)(2,1)S(1)} all-gather(bf16[192,256]{1,0:T(8,128)(2,1)S(1)} %copy-done.2), channel_id=1, replica_groups=mesh['ep'=8,'tp'=4] {'ep'}, dimensions={0}, use_global_device_ids=true | all-gather | bytes 884736 | tf_op jit(solution)/shard_map/all_gather | solution.py:77
  186.0 1.2 copy.45
  187.1 0.0 copy-done.3
  187.1 0.0 copy-start.4
  187.1 0.1 copy.44
  187.2 37.0 %reduce-scatter.5.cloned.1.call-done = bf16[512,2048]{1,0:T(8,128)(2,1)} async-done(((bf16[2048,2048]{1,0:T(8,128)(2,1)}), bf16[512,2048]{1,0:T(8,128)(2,1)}) %reduce-scatter.5.cloned.1.call-update) | async-done | bytes 2097168 | tf_op jit(solution)/shard_map/reduce_scatter | solution.py:132
  224.2 5.5 %all-to-all-start.1 = ((bf16[8,64,2048]{2,1,0:T(8,128)(2,1)}), bf16[8,64,2048]{2,1,0:T(8,128)(2,1)S(1)}, u32[]{:S(2)}, u32[]{:S(2)}) async-start(bf16[8,64,2048]{2,1,0:T(8,128)(2,1)} %bitcast.79), calls=%async_computation.3 | async-start | bytes 4194304 | tf_op jit(solution)/shard_map/all_to_all | solution.py:138
  229.7 0.0 reduce-scatter.3.cloned.1.call-start
  229.8 0.0 copy-done.4
  229.8 71.9 %all_gather.10 = bf16[1536,256]{1,0:T(8,128)(2,1)} all-gather(bf16[192,256]{1,0:T(8,128)(2,1)S(1)} %copy-done.4), channel_id=1, replica_groups=mesh['ep'=8,'tp'=4] {'ep'}, dimensions={0}, use_global_device_ids=true | all-gather | bytes 884736 | tf_op jit(solution)/shard_map/all_gather | solution.py:78
  301.7 2.3 copy.46
  304.0 2.0 multiply_reduce_fusion
  306.1 0.0 copy-start.1
  306.1 0.9 fusion
  307.0 0.2 copy-done.1
  307.2 0.0 copy-start.7
  307.2 0.0 copy-start.8
  307.2 1.2 fusion.23
  308.4 0.0 copy-done.7
  308.4 0.0 copy-start.5
  308.4 0.0 copy-start.6
  308.5 0.2 multiply_reduce_fusion.2
  308.7 0.0 copy-done.8
  308.7 2.6 convolution_convert_fusion.1
  311.3 0.0 reduce-scatter.3.cloned.1.call-update
  311.3 0.0 copy-done.5
  311.3 0.0 copy-done.6
  311.5 0.1 copy.50
  311.6 0.0 all-to-all-done.1
  311.6 2.3 gather_fusion
  314.0 2.4 reshape.260
  316.4 3.9 %multiply_reduce_fusion.1 = bf16[128,2048]{1,0:T(8,128)(2,1)} fusion(f32[128,2,2048]{2,1,0:T(2,128)S(1)} %reshape.260, f32[128,2]{1,0:T(8,128)S(1)} %copy.50), kind=kLoop, calls=%fused_computation.14 | loop fusion | flops 786432 | bytes 2622464 | tf_op jit(solution)/shard_map/reduce_sum | solution.py:158
  320.3 12.9 %reduce-scatter.3.cloned.1.call-done = bf16[48,2048]{1,0:T(8,128)(2,1)} async-done(((bf16[192,2048]{1,0:T(8,128)(2,1)}), bf16[48,2048]{1,0:T(8,128)(2,1)}) %reduce-scatter.3.cloned.1.call-update) | async-done | bytes 196624 | tf_op jit(solution)/shard_map/reduce_scatter | solution.py:98
  (19 shorter events, 0.3 us)
Async XLA Ops:
  7.2 132.3 %copy-start = (bf16[1,256,2048]{2,1,0:T(8,128)(2,1)S(1)}, bf16[1,256,2048]{2,1,0:T(8,128)(2,1)}, u32[]{:S(2)}) copy-start(bf16[1,256,2048]{2,1,0:T(8,128)(2,1)} %param.27) | copy-start | bytes 3145732
  7.2 124.9 %all-gather.2.cloned.1.call-start = ((), (), s32[]{:S(2)}) async-start(), calls=%async_computation.5 | async-start | bytes 10485760 | tf_op jit(solution)/shard_map/all_gather | solution.py:128
  74.6 149.6 %reduce-scatter.5.cloned.1.call-start = ((), (), s32[]{:S(2)}) async-start(), calls=%async_computation.6 | async-start | bytes 10485760 | tf_op jit(solution)/shard_map/reduce_scatter | solution.py:132
  132.1 7.4 %copy-start.9 = (bf16[1,2048,256]{2,1,0:T(8,128)(2,1)S(1)}, bf16[1,2048,256]{2,1,0:T(8,128)(2,1)}, u32[]{:S(2)}) copy-start(bf16[1,2048,256]{2,1,0:T(8,128)(2,1)} %param.26) | copy-start | bytes 3145732
  152.7 0.9 copy-start.2
  153.5 33.6 %copy-start.3 = (bf16[192,256]{1,0:T(8,128)(2,1)S(1)}, bf16[192,256]{1,0:T(8,128)(2,1)}, u32[]{:S(2)}) copy-start(bf16[192,256]{1,0:T(8,128)(2,1)} %param.14) | copy-start | bytes 294916
  187.1 42.6 %copy-start.4 = (bf16[192,256]{1,0:T(8,128)(2,1)S(1)}, bf16[192,256]{1,0:T(8,128)(2,1)}, u32[]{:S(2)}) copy-start(bf16[192,256]{1,0:T(8,128)(2,1)} %param.16) | copy-start | bytes 294916
  224.2 87.4 %all-to-all-start.1 = ((bf16[8,64,2048]{2,1,0:T(8,128)(2,1)}), bf16[8,64,2048]{2,1,0:T(8,128)(2,1)S(1)}, u32[]{:S(2)}, u32[]{:S(2)}) async-start(bf16[8,64,2048]{2,1,0:T(8,128)(2,1)} %bitcast.79), calls=%async_computation.3 | async-start | bytes 4194304 | tf_op jit(solution)/shard_map/all_to_all | solution.py:138
  229.7 103.5 %reduce-scatter.3.cloned.1.call-start = ((), (), s32[]{:S(2)}) async-start(), calls=%async_computation.4 | async-start | bytes 983040 | tf_op jit(solution)/shard_map/reduce_scatter | solution.py:98
  306.1 1.1 copy-start.1
  307.2 1.2 copy-start.7
  307.2 1.5 copy-start.8
  308.4 2.9 copy-start.5
  308.4 2.9 copy-start.6
Sparse Core Ops, SparseCore 0:
  74.7 57.2 all-gather.1
  152.8 71.3 reduce-scatter.4
  311.4 21.7 reduce-scatter.2
where the time goes:
time: 340 us
  blocking collectives  160 us (47%)
  waiting for transfers between devices  107 us (31%)
  matrix products  26.4 us (8%)
  local copies, waits for them, and re-layouts  16.6 us (5%)
  between operations  14 us (4%)
  other arithmetic  10 us (3%)
  starting transfers between devices  5.81 us (2%)
    all_gather x1, blocking collectives, local(): value_piece = lax.all_gather(value_rows, 'ep', axis=0, tiled=True)  71.9 us
    all_gather x1, waiting for transfers between devices, local(): pieces = lax.all_gather(arrived, 'tp', axis=0, tiled=True)  57.2 us
    all_to_all x1, blocking collectives, local(): lax.all_to_all(outgoing.reshape(expert_count, capacity, model_width), 'ep...  55.4 us
    reduce_scatter x1, waiting for transfers between devices, local(): lax.psum_scatter(jnp.dot(hidden_flat, w_down[0], preferred_element_type=j...  37 us
    all_gather x1, blocking collectives, local(): key_piece = lax.all_gather(key_rows, 'ep', axis=0, tiled=True)  32.4 us
    dot_general x1, matrix products, local(): jnp.dot(hidden_flat, w_down[0], preferred_element_type=jnp.float32)  13.2 us
    reduce_scatter x1, waiting for transfers between devices, local(): lax.psum_scatter(jnp.dot(attended, own_weight, preferred_element_type=jnp...  12.9 us
    dot_general x1, matrix products, expert_hidden(): jnp.dot(arrived, gate_weight, preferred_element_type=jnp.float32)  7.4 us
  transfers between devices with their start and end apart: 4, of which 3 were waited for; matrix products, arithmetic and copies ran while one was open for 6% of the time, Pallas kernels for 0%

commit v1 on v0

--- a/solution.py
+++ b/solution.py
@@ -75,7 +75,14 @@
     )
     carried = start_state
     key_piece = lax.all_gather(key_rows, "ep", axis=0, tiled=True)
-    value_piece = lax.all_gather(value_rows, "ep", axis=0, tiled=True)
+    n_dev = lax.axis_size("ep")
+    right = [(i, (i + 1) % n_dev) for i in range(n_dev)]
+    parts = [value_rows]
+    for stride in range(1, n_dev):
+        parts = [lax.ppermute(parts[0], "ep", right), *parts]
+    result = jnp.concatenate(parts, axis=0)
+    shift = (lax.axis_index("ep") + 1) * parts[-1].shape[0]
+    value_piece = jnp.roll(result, shift, axis=0)
     length = key_piece.shape[0]
     block_rows = 1024 if length % 1024 == 0 else length
     blocks = (

time: 340 us -> 333 us (0.979)
  blocking collectives: 160 us -> 88.8 us
  waiting for transfers between devices: 107 us -> 160 us
  starting transfers between devices: 5.81 us -> 10.1 us
  local copies, waits for them, and re-layouts: 16.6 us -> 20.2 us
    all_gather x1 -> x0, blocking collectives: 71.9 us -> none  [local(): value_piece = lax.all_gather(value_rows, 'ep', axis=0, tiled=True)]
    ppermute x0 -> x7, waiting for transfers between devices: none -> 66.4 us  [local(): parts = [lax.ppermute(parts[0], 'ep', right), *parts]]
    reduce_scatter x1, waiting for transfers between devices: 37 us -> 18.5 us  [local(): lax.psum_scatter(jnp.dot(hidden_flat, w_down[0], preferred_element_type=j...]
    reduce_scatter x1, waiting for transfers between devices: 12.9 us -> 17.5 us  [local(): lax.psum_scatter(jnp.dot(attended, own_weight, preferred_element_type=jnp...]
    ppermute x0 -> x7, starting transfers between devices: none -> 4.29 us  [local(): parts = [lax.ppermute(parts[0], 'ep', right), *parts]]
    concatenate x0 -> x1, local copies, waits for them, and re-layouts: none -> 3.84 us  [local(): value_piece = jnp.roll(result, shift, axis=0)]
  transfers between devices with their start and end apart: 4 -> 11, of which waited for: 3 -> 8; matrix products, arithmetic and copies ran while one was open for 6% -> 8% of each run, Pallas kernels for 0% -> 0%
where the time goes in v1:
time: 333 us; the launch traced here: 332 us
  waiting for transfers between devices  160 us (48%)
  blocking collectives  88.8 us (27%)
  matrix products  28.6 us (9%)
  local copies, waits for them, and re-layouts  20.2 us (6%)
  between operations  14 us (4%)
  other arithmetic  10.6 us (3%)
  starting transfers between devices  10.1 us (3%)
    ppermute x7, waiting for transfers between devices, local(): parts = [lax.ppermute(parts[0], 'ep', right), *parts]  66.4 us
    all_gather x1, waiting for transfers between devices, local(): pieces = lax.all_gather(arrived, 'tp', axis=0, tiled=True)  57.2 us
    all_to_all x1, blocking collectives, local(): lax.all_to_all(outgoing.reshape(expert_count, capacity, model_width), 'ep...  55.4 us
    all_gather x1, blocking collectives, local(): key_piece = lax.all_gather(key_rows, 'ep', axis=0, tiled=True)  33.4 us
    reduce_scatter x1, waiting for transfers between devices, local(): lax.psum_scatter(jnp.dot(hidden_flat, w_down[0], preferred_element_type=j...  18.5 us
    reduce_scatter x1, waiting for transfers between devices, local(): lax.psum_scatter(jnp.dot(attended, own_weight, preferred_element_type=jnp...  17.5 us
    dot_general x1, matrix products, local(): jnp.dot(hidden_flat, w_down[0], preferred_element_type=jnp.float32)  13.2 us
    dot_general x1, matrix products, expert_hidden(): jnp.dot(arrived, gate_weight, preferred_element_type=jnp.float32)  7.4 us
  transfers between devices with their start and end apart: 11, of which 8 were waited for; matrix products, arithmetic and copies ran while one was open for 8% of the time, Pallas kernels for 0%

profile of v1, /device:TPU:0, one launch (start us, length us, event | category | flops | bytes accessed | tf_op | source)
XLA Modules:
  0.0 332.0 jit_solution(13104202362934468836)
XLA Ops:
  7.2 0.0 copy-start
  7.2 0.0 all-gather.2.cloned.1.call-start
  7.2 0.8 and_select_fusion
  8.0 0.1 copy.58
  8.1 0.1 eq.46
  8.3 0.6 reduce-window.6
  8.9 0.2 slice_reduce_fusion
  9.1 0.1 fusion.32
  9.2 0.1 copy.57
  9.3 0.1 mul.156
  9.5 0.1 reshape.255
  9.6 1.2 fusion.10
  10.9 2.0 fusion.12
  12.9 6.2 %scatter_custom_fusion = bf16[512,2048]{1,0:T(8,128)(2,1)S(1)} fusion(s32[256]{0:T(256)S(1)} %bitcast.82, bf16[128,2048]{1,0:T(8,128)(2,1)} %fusion.12, s32[1024]{0:T(1024)S(1)} %pad_clamp_fusion.1, bf16[]{:T(256)} %constant.99.clone.1), kind=kCustom, calls=%fused_computation.25 | custom fusion | bytes 2097664 | tf_op jit(solution)/shard_map/scatter | solution.py:126
  19.2 55.4 %all_to_all.10 = bf16[8,64,2048]{2,1,0:T(8,128)(2,1)} all-to-all(bf16[8,64,2048]{2,1,0:T(8,128)(2,1)S(1)} %bitcast.77), channel_id=1, replica_groups=mesh['ep'=8,'tp'=4] {'ep'}, dimensions={0} | all-to-all | bytes 4194304 | tf_op jit(solution)/shard_map/all_to_all | solution.py:128
  74.6 0.0 all-gather.2.cloned.1.call-update
  74.6 0.2 reduce-scatter.5.cloned.1.call-start
  74.9 57.2 %all-gather.2.cloned.1.call-done = bf16[32,64,2048]{2,1,0:T(8,128)(2,1)} async-done(((bf16[8,64,2048]{2,1,0:T(8,128)(2,1)}), bf16[32,64,2048]{2,1,0:T(8,128)(2,1)}) %all-gather.2.cloned.1.call-update) | async-done | bytes 8388624 | tf_op jit(solution)/shard_map/all_gather | solution.py:135
  132.1 7.4 %fusion.16 = f32[2048,256]{1,0:T(8,128)} fusion(bf16[2048,2048]{1,0:T(8,128)(2,1)} %bitcast.87, bf16[1,2048,256]{2,1,0:T(8,128)(2,1)} %param.25), kind=kOutput, calls=%fused_computation.23 | convolution fusion | flops 2147483648 | bytes 11534336 | tf_op jit(solution)/shard_map/dot_general | solution.py:24
  139.5 13.2 %convolution_convert_fusion = bf16[2048,2048]{1,0:T(8,128)(2,1)} fusion(bf16[2048,2048]{1,0:T(8,128)(2,1)} %bitcast.88, f32[2048,256]{1,0:T(8,128)} %fusion.16, bf16[1,256,2048]{2,1,0:T(8,128)(2,1)S(1)} %copy-done, bf16[1,2048,256]{2,1,0:T(8,128)(2,1)S(1)} %copy-done.10), kind=kOutput, calls=%fused_computation.3 | convolution fusion | flops 4302307328 | bytes 20971520 | tf_op jit(solution)/shard_map/dot_general | solution.py:140
  152.7 0.0 reduce-scatter.5.cloned.1.call-update
  152.7 0.9 copy-done.3
  153.6 0.1 copy.50
  153.7 1.5 collective-permute-start
  155.2 6.9 %collective-permute-done = bf16[192,256]{0,1:T(8,128)(2,1)S(1)} collective-permute-done((bf16[192,256]{0,1:T(8,128)(2,1)S(1)}, bf16[192,256]{0,1:T(8,128)(2,1)S(1)}, u32[]{:S(2)}, u32[]{:S(2)}) %collective-permute-start) | collective-permute-done | bytes 98336 | tf_op jit(solution)/shard_map/ppermute | solution.py:82
  162.1 0.0 collective-permute-start.1
  162.1 7.7 %collective-permute-done.1 = bf16[192,256]{0,1:T(8,128)(2,1)S(1)} collective-permute-done((bf16[192,256]{0,1:T(8,128)(2,1)S(1)}, bf16[192,256]{0,1:T(8,128)(2,1)S(1)}, u32[]{:S(2)}, u32[]{:S(2)}) %collective-permute-start.1) | collective-permute-done | bytes 98336 | tf_op jit(solution)/shard_map/ppermute | solution.py:82
  169.7 0.0 collective-permute-start.2
  169.7 33.4 %all_gather.6 = bf16[1536,256]{1,0:T(8,128)(2,1)S(1)} all-gather(bf16[192,256]{1,0:T(8,128)(2,1)S(1)} %copy-done.4), channel_id=1, replica_groups=mesh['ep'=8,'tp'=4] {'ep'}, dimensions={0}, use_global_device_ids=true | all-gather | bytes 884736 | tf_op jit(solution)/shard_map/all_gather | solution.py:77
  203.1 1.2 copy.49
  204.3 0.8 copy.48
  205.0 0.0 collective-permute-done.2
  205.0 0.7 collective-permute-start.3
  205.8 18.5 %reduce-scatter.5.cloned.1.call-done = bf16[512,2048]{1,0:T(8,128)(2,1)} async-done(((bf16[2048,2048]{1,0:T(8,128)(2,1)}), bf16[512,2048]{1,0:T(8,128)(2,1)}) %reduce-scatter.5.cloned.1.call-update) | async-done | bytes 2097168 | tf_op jit(solution)/shard_map/reduce_scatter | solution.py:139
  224.2 5.5 %all-to-all-start.1 = ((bf16[8,64,2048]{2,1,0:T(8,128)(2,1)}), bf16[8,64,2048]{2,1,0:T(8,128)(2,1)S(1)}, u32[]{:S(2)}, u32[]{:S(2)}) async-start(bf16[8,64,2048]{2,1,0:T(8,128)(2,1)} %bitcast.79), calls=%async_computation.3 | async-start | bytes 4194304 | tf_op jit(solution)/shard_map/all_to_all | solution.py:145
  229.7 0.0 reduce-scatter.3.cloned.1.call-start
  229.8 2.1 multiply_reduce_fusion
  231.9 0.0 collective-permute-done.3
  231.9 2.0 collective-permute-start.4
  234.0 37.4 %collective-permute-done.4 = bf16[192,256]{0,1:T(8,128)(2,1)S(1)} collective-permute-done((bf16[192,256]{0,1:T(8,128)(2,1)}, bf16[192,256]{0,1:T(8,128)(2,1)S(1)}, u32[]{:S(2)}, u32[]{:S(2)}) %collective-permute-start.4) | collective-permute-done | bytes 98336 | tf_op jit(solution)/shard_map/ppermute | solution.py:82
  271.4 0.0 collective-permute-start.5
  271.4 0.9 fusion
  272.3 6.9 %collective-permute-done.5 = bf16[192,256]{0,1:T(8,128)(2,1)} collective-permute-done((bf16[192,256]{0,1:T(8,128)(2,1)S(1)}, bf16[192,256]{0,1:T(8,128)(2,1)}, u32[]{:S(2)}, u32[]{:S(2)}) %collective-permute-start.5) | collective-permute-done | bytes 98336 | tf_op jit(solution)/shard_map/ppermute | solution.py:82
  279.2 0.0 collective-permute-start.6
  279.2 0.6 exponential_multiply_fusion
  279.8 7.5 %collective-permute-done.6 = bf16[192,256]{0,1:T(8,128)(2,1)} collective-permute-done((bf16[192,256]{0,1:T(8,128)(2,1)}, bf16[192,256]{0,1:T(8,128)(2,1)}, u32[]{:S(2)}, u32[]{:S(2)}) %collective-permute-start.6) | collective-permute-done | bytes 98336 | tf_op jit(solution)/shard_map/ppermute | solution.py:82
  287.3 3.8 %concatenate.6 = bf16[3072,256]{0,1:T(8,128)(2,1)} concatenate(bf16[192,256]{0,1:T(8,128)(2,1)} %collective-permute-done.6, bf16[192,256]{0,1:T(8,128)(2,1)} %collective-permute-done.5, bf16[192,256]{0,1:T(8,128)(2,1)} %copy-done.2, bf16[192,256]{0,1:T(8,128)(2,1)} %collective-permute-done.3, bf16[192,256]{0,1:T(8,128)(2,1)} %collective-permute-done.2, ...), dimensions={0} | concatenate | bytes 3145728 | tf_op jit(solution)/shard_map/jit(_roll_dynamic)/concatenate | solution.py:85
  291.2 1.5 constant_dynamic-slice_fusion.3
  292.6 0.0 copy-start.8
  292.6 0.0 copy-start.9
  292.7 3.4 %fusion.23 = f32[2,2,192,128]{3,2,1,0:T(8,128)S(1)} fusion(bf16[1536,2,128,1]{0,2,3,1:T(8,128)(2,1)S(1)} %bitcast.80, f32[2,2,192,1536]{3,2,1,0:T(8,128)} %copy-done.1, f32[2,2,192]{2,1,0:T(2,128)S(1)} %broadcast_maximum_fusion, f32[2,2,192]{2,1,0:T(2,128)} %get-tuple-element.19, f32[2,2,192]{2,1,0:T(2,128)S(1)} %get-tuple-element.18), kind=kOutput, calls=%fused_computation.30 | convolution fusion | flops 305725440 | bytes 5907456 | tf_op jit(solution)/shard_map/while/body/eval_jaxpr/hmqk,khv->hmqv/dot_general | solution.py:63
  296.0 0.0 copy-done.8
  296.0 0.0 copy-start.6
  296.0 0.0 copy-start.7
  296.1 0.2 multiply_reduce_fusion.2
  296.3 2.6 convolution_convert_fusion.1
  298.9 0.0 reduce-scatter.3.cloned.1.call-update
  298.9 0.0 copy-done.6
  299.1 0.1 copy.56
  299.2 0.0 all-to-all-done.1
  299.2 2.3 gather_fusion
  301.6 2.4 reshape.260
  304.0 3.9 %multiply_reduce_fusion.1 = bf16[128,2048]{1,0:T(8,128)(2,1)} fusion(f32[128,2,2048]{2,1,0:T(2,128)S(1)} %reshape.260, f32[128,2]{1,0:T(8,128)S(1)} %copy.56), kind=kLoop, calls=%fused_computation.14 | loop fusion | flops 786432 | bytes 2622464 | tf_op jit(solution)/shard_map/reduce_sum | solution.py:165
  307.9 17.5 %reduce-scatter.3.cloned.1.call-done = bf16[48,2048]{1,0:T(8,128)(2,1)} async-done(((bf16[192,2048]{1,0:T(8,128)(2,1)}), bf16[48,2048]{1,0:T(8,128)(2,1)}) %reduce-scatter.3.cloned.1.call-update) | async-done | bytes 196624 | tf_op jit(solution)/shard_map/reduce_scatter | solution.py:105
  (32 shorter events, 0.3 us)
Async XLA Ops:
  7.2 132.3 %copy-start = (bf16[1,256,2048]{2,1,0:T(8,128)(2,1)S(1)}, bf16[1,256,2048]{2,1,0:T(8,128)(2,1)}, u32[]{:S(2)}) copy-start(bf16[1,256,2048]{2,1,0:T(8,128)(2,1)} %param.27) | copy-start | bytes 3145732
  7.2 124.9 %all-gather.2.cloned.1.call-start = ((), (), s32[]{:S(2)}) async-start(), calls=%async_computation.5 | async-start | bytes 10485760 | tf_op jit(solution)/shard_map/all_gather | solution.py:135
  74.6 149.6 %reduce-scatter.5.cloned.1.call-start = ((), (), s32[]{:S(2)}) async-start(), calls=%async_computation.6 | async-start | bytes 10485760 | tf_op jit(solution)/shard_map/reduce_scatter | solution.py:139
  132.1 7.4 %copy-start.10 = (bf16[1,2048,256]{2,1,0:T(8,128)(2,1)S(1)}, bf16[1,2048,256]{2,1,0:T(8,128)(2,1)}, u32[]{:S(2)}) copy-start(bf16[1,2048,256]{2,1,0:T(8,128)(2,1)} %param.26) | copy-start | bytes 3145732
  152.7 0.9 copy-start.3
  152.7 17.1 %copy-start.4 = (bf16[192,256]{1,0:T(8,128)(2,1)S(1)}, bf16[192,256]{1,0:T(8,128)(2,1)}, u32[]{:S(2)}) copy-start(bf16[192,256]{1,0:T(8,128)(2,1)} %param.15) | copy-start | bytes 294916
  153.5 50.7 %copy-start.5 = (bf16[192,256]{1,0:T(8,128)(2,1)S(1)}, bf16[192,256]{1,0:T(8,128)(2,1)}, u32[]{:S(2)}) copy-start(bf16[192,256]{1,0:T(8,128)(2,1)} %param.14) | copy-start | bytes 294916
  153.7 8.4 %collective-permute-start = (bf16[192,256]{0,1:T(8,128)(2,1)S(1)}, bf16[192,256]{0,1:T(8,128)(2,1)S(1)}, u32[]{:S(2)}, u32[]{:S(2)}) collective-permute-start(bf16[192,256]{0,1:T(8,128)(2,1)S(1)} %copy.50), channel_id=1, source_target_pairs={{0,4},{4,8},{8,12},{12,16},{16,20},{20,24},{24,28},{28,0},{1,5},{5... | collective-permute-start | bytes 294920 | tf_op jit(solution)/shard_map/ppermute | solution.py:82
  162.1 7.7 %collective-permute-start.1 = (bf16[192,256]{0,1:T(8,128)(2,1)S(1)}, bf16[192,256]{0,1:T(8,128)(2,1)S(1)}, u32[]{:S(2)}, u32[]{:S(2)}) collective-permute-start(bf16[192,256]{0,1:T(8,128)(2,1)S(1)} %collective-permute-done), channel_id=1, source_target_pairs={{0,4},{4,8},{8,12},{12,16},{16,20},{20,24},{24,28},{28,0},{1,5},{5... | collective-permute-start | bytes 294920 | tf_op jit(solution)/shard_map/ppermute | solution.py:82
  169.7 35.3 %collective-permute-start.2 = (bf16[192,256]{0,1:T(8,128)(2,1)S(1)}, bf16[192,256]{0,1:T(8,128)(2,1)}, u32[]{:S(2)}, u32[]{:S(2)}) collective-permute-start(bf16[192,256]{0,1:T(8,128)(2,1)S(1)} %collective-permute-done.1), channel_id=1, source_target_pairs={{0,4},{4,8},{8,12},{12,16},{16,20},{20,24},{24,28},{28,0},{1,5},{5... | collective-permute-start | bytes 294920 | tf_op jit(solution)/shard_map/ppermute | solution.py:82
  205.0 26.9 %collective-permute-start.3 = (bf16[192,256]{0,1:T(8,128)(2,1)}, bf16[192,256]{0,1:T(8,128)(2,1)}, u32[]{:S(2)}, u32[]{:S(2)}) collective-permute-start(bf16[192,256]{0,1:T(8,128)(2,1)} %collective-permute-done.2), channel_id=1, source_target_pairs={{0,4},{4,8},{8,12},{12,16},{16,20},{20,24},{24,28},{28,0},{1,5},{5... | collective-permute-start | bytes 294920 | tf_op jit(solution)/shard_map/ppermute | solution.py:82
  224.2 75.0 %all-to-all-start.1 = ((bf16[8,64,2048]{2,1,0:T(8,128)(2,1)}), bf16[8,64,2048]{2,1,0:T(8,128)(2,1)S(1)}, u32[]{:S(2)}, u32[]{:S(2)}) async-start(bf16[8,64,2048]{2,1,0:T(8,128)(2,1)} %bitcast.79), calls=%async_computation.3 | async-start | bytes 4194304 | tf_op jit(solution)/shard_map/all_to_all | solution.py:145
  229.7 95.7 %reduce-scatter.3.cloned.1.call-start = ((), (), s32[]{:S(2)}) async-start(), calls=%async_computation.4 | async-start | bytes 983040 | tf_op jit(solution)/shard_map/reduce_scatter | solution.py:105
  231.9 40.4 %copy-start.1 = (f32[2,2,192,1536]{3,2,1,0:T(8,128)}, f32[2,2,192,1536]{3,2,1,0:T(8,128)S(1)}, u32[]{:S(2)}) copy-start(f32[2,2,192,1536]{3,2,1,0:T(8,128)S(1)} %get-tuple-element.28) | copy-start | bytes 14155780
  231.9 39.4 %collective-permute-start.4 = (bf16[192,256]{0,1:T(8,128)(2,1)}, bf16[192,256]{0,1:T(8,128)(2,1)S(1)}, u32[]{:S(2)}, u32[]{:S(2)}) collective-permute-start(bf16[192,256]{0,1:T(8,128)(2,1)} %collective-permute-done.3), channel_id=1, source_target_pairs={{0,4},{4,8},{8,12},{12,16},{16,20},{20,24},{24,28},{28,0},{1,5},{5... | collective-permute-start | bytes 294920 | tf_op jit(solution)/shard_map/ppermute | solution.py:82
  271.4 7.9 %copy-start.2 = (bf16[192,256]{0,1:T(8,128)(2,1)}, bf16[192,256]{0,1:T(8,128)(2,1)S(1)}, u32[]{:S(2)}) copy-start(bf16[192,256]{0,1:T(8,128)(2,1)S(1)} %collective-permute-done.4) | copy-start | bytes 294916
  271.4 7.9 %collective-permute-start.5 = (bf16[192,256]{0,1:T(8,128)(2,1)S(1)}, bf16[192,256]{0,1:T(8,128)(2,1)}, u32[]{:S(2)}, u32[]{:S(2)}) collective-permute-start(bf16[192,256]{0,1:T(8,128)(2,1)S(1)} %collective-permute-done.4), channel_id=1, source_target_pairs={{0,4},{4,8},{8,12},{12,16},{16,20},{20,24},{24,28},{28,0},{1,5},{5... | collective-permute-start | bytes 294920 | tf_op jit(solution)/shard_map/ppermute | solution.py:82
  279.2 8.1 %collective-permute-start.6 = (bf16[192,256]{0,1:T(8,128)(2,1)}, bf16[192,256]{0,1:T(8,128)(2,1)}, u32[]{:S(2)}, u32[]{:S(2)}) collective-permute-start(bf16[192,256]{0,1:T(8,128)(2,1)} %collective-permute-done.5), channel_id=1, source_target_pairs={{0,4},{4,8},{8,12},{12,16},{16,20},{20,24},{24,28},{28,0},{1,5},{5... | collective-permute-start | bytes 294920 | tf_op jit(solution)/shard_map/ppermute | solution.py:82
  292.6 3.4 %copy-start.8 = (f32[2]{0:T(128)S(1)}, f32[2]{0:T(128)}, u32[]{:S(2)}) copy-start(f32[2]{0:T(128)} %param.17) | copy-start | bytes 28
  292.6 3.6 %copy-start.9 = (f32[128]{0:T(128)S(1)}, f32[128]{0:T(128)}, u32[]{:S(2)}) copy-start(f32[128]{0:T(128)} %param.18) | copy-start | bytes 1540
  296.0 2.9 copy-start.6
  296.0 2.9 copy-start.7
Sparse Core Ops, SparseCore 0:
  74.7 57.2 all-gather.1
  152.8 71.3 reduce-scatter.4
  299.0 26.3 reduce-scatter.2
